TPU v7x, 32 devices: a whole 2x2x4 slice. The times are simulated.
32 devices in a mesh: sp: 8 (over z, x), tp: 4 (over y, core).
Axes of the slice: x: 2, y: 2, z: 4, core: 2. Of those that a mesh axis runs over, the one named last changes fastest.
Arguments:
- tokens: bfloat16 [2048, 2048], P(('sp', 'tp')), may hold values from -40 to 40
- w_query: bfloat16 [2048, 1024], P(None, 'tp'), may hold values from -0.125 to 0.125
- w_key: bfloat16 [2048, 256], P(None, 'tp'), may hold values from -0.125 to 0.125
- w_value: bfloat16 [2048, 256], P(None, 'tp'), may hold values from -0.125 to 0.125
- w_out: bfloat16 [1024, 2048], P('tp'), may hold values from -0.1875 to 0.1875
- cum_gate: float32 [16, 2048], P('tp', 'sp'), may hold values from -295 to 0, as said below
Outputs:
- layer_out: bfloat16 [2048, 2048], P(('sp', 'tp'))
Inputs may be any that keep to these rules, and one draw needn't show every extreme that they name: `cum_gate`: each head's row does not rise along the positions.
All inputs are finite; a program needn't handle non-finite values.
Results may differ from a plain program's by a relative error of at most 0.012.
Values may be sent and summed in bfloat16 or wider, within the bound.
A program may use at most 64 MiB of HBM per device.

v0:
```python
import math
import jax
import jax.numpy as jnp
from jax import lax
from jax.sharding import PartitionSpec as P

HD = 64


def per_device(tokens, w_query, w_key, w_value, w_out, cum_gate):
    pieces = lax.all_gather(tokens, "tp", axis=0, tiled=True)
    query_part = jnp.dot(pieces, w_query, preferred_element_type=jnp.float32).astype(jnp.bfloat16)
    key_part = jnp.dot(pieces, w_key, preferred_element_type=jnp.float32).astype(jnp.bfloat16)
    value_part = jnp.dot(pieces, w_value, preferred_element_type=jnp.float32).astype(jnp.bfloat16)
    projected = jnp.concatenate([query_part, key_part, value_part], axis=1)
    row_count = projected.shape[0]
    heads_local = w_query.shape[1] // HD
    kv_local = w_key.shape[1] // HD
    group_size = heads_local // kv_local
    score_factor = float(HD) ** (-0.5)
    query_flat = projected[:, : heads_local * HD]
    key_values = projected[:, heads_local * HD :]
    first_pos = lax.axis_index("sp") * row_count
    own_pos = first_pos + jnp.arange(row_count, dtype=jnp.int32)
    gate_all = lax.all_gather(cum_gate, "sp", axis=1, tiled=True)
    groups = (query_flat, cum_gate, own_pos)
    prepared = []
    query_rows, query_gates, query_pos = groups
    count = query_rows.shape[0]
    prepared.append(
        (
            query_rows.reshape(count, kv_local, group_size, HD),
            query_gates.reshape(kv_local, group_size, count, 1),
            query_pos,
            jnp.max(query_pos),
        )
    )
    initial = tuple(
        (
            (
                jnp.full((kv_local, group_size, member[2].shape[0]), -1e30, jnp.float32),
                jnp.zeros((kv_local, group_size, member[2].shape[0]), jnp.float32),
                jnp.zeros((kv_local, group_size, member[2].shape[0], HD), jnp.float32),
            )
            for member in prepared
        )
    )
    pieces = lax.all_gather(key_values, "sp", axis=0, tiled=True)
    piece_rows = pieces.shape[0]
    key_block = math.gcd(piece_rows, 1024)

    def one_block(index, hidden_vectors):
        block_start = index * key_block
        slab = lax.dynamic_slice_in_dim(pieces, block_start, key_block, 0)
        key_rows = slab[:, : kv_local * HD].reshape(key_block, kv_local, HD)
        value_rows = slab[:, kv_local * HD :].reshape(key_block, kv_local, HD)
        key_cum = lax.dynamic_slice_in_dim(gate_all, block_start, key_block, 1)
        key_cum = key_cum.reshape(kv_local, group_size, 1, key_block)
        key_pos = block_start + jnp.arange(key_block, dtype=jnp.int32)
        results = []
        for member, state in zip(prepared, hidden_vectors):
            queries, query_cum, query_pos, last_pos = member

            def compute(inner, queries=queries, query_cum=query_cum, query_pos=query_pos):
                top_score, weight_sum, accumulated = inner
                scores = (
                    jnp.einsum(
                        "tkgd,skd->kgts", queries, key_rows, preferred_element_type=jnp.float32
                    )
                    * score_factor
                )
                scores = scores + (query_cum - key_cum)
                scores = jnp.where(key_pos[None, :] <= query_pos[:, None], scores, -jnp.inf)
                new_top = jnp.maximum(top_score, jnp.max(scores, axis=-1))
                weights = jnp.exp(scores - new_top[..., None])
                decay = jnp.exp(top_score - new_top)
                weight_sum = weight_sum * decay + jnp.sum(weights, axis=-1)
                update = jnp.einsum(
                    "kgts,skd->kgtd",
                    weights.astype(jnp.bfloat16),
                    value_rows,
                    preferred_element_type=jnp.float32,
                )
                accumulated = accumulated * decay[..., None] + update
                return (new_top, weight_sum, accumulated)

            def skipped(inner):
                return inner

            results.append(lax.cond(block_start <= last_pos, compute, skipped, state))
        return tuple(results)

    finals = lax.fori_loop(0, piece_rows // key_block, one_block, initial)
    parts = []
    for top_score, weight_sum, accumulated in finals:
        count = weight_sum.shape[2]
        rows = (accumulated / weight_sum[..., None]).astype(jnp.bfloat16)
        parts.append(rows.transpose(2, 0, 1, 3).reshape(count, heads_local * HD))
    attended = parts[0]
    regrouped = lax.all_to_all(attended, "tp", split_axis=0, concat_axis=1, tiled=True)
    summed = jnp.dot(
        regrouped,
        lax.all_gather(w_out, "tp", axis=0, tiled=True),
        preferred_element_type=jnp.float32,
    )
    return summed.astype(jnp.bfloat16)


def solution(mesh):
    placed = (
        P(("sp", "tp"), None),
        P(None, "tp"),
        P(None, "tp"),
        P(None, "tp"),
        P("tp", None),
        P("tp", "sp"),
    )
    return jax.shard_map(
        per_device, mesh=mesh, in_specs=placed, out_specs=P(("sp", "tp"), None), check_vma=False
    )
```

profile of v0, /device:TPU:26, one launch (start us, length us, event | category | flops | bytes accessed | tf_op | source)
XLA Modules:
  0.0 111.5 jit_solution(12001325183075027937)
XLA Ops:
  6.5 0.7 all-gather.3.cloned.1.call-update
  7.3 0.0 all-gather.5.cloned.1.call-start
  7.3 0.7 all-gather.5.cloned.1.call-update
  8.0 0.7 add_reduce_fusion
  8.7 30.7 %all_gather.14 = f32[4,2048]{1,0:T(4,128)S(1)} all-gather(f32[4,256]{1,0:T(4,128)} %param.15), channel_id=1, replica_groups=mesh['sp'=8,'tp'=4] {'sp'}, dimensions={1}, use_global_device_ids=true | all-gather | bytes 36864 | tf_op jit(solution)/shard_map/all_gather | solution.py:25
  39.4 1.7 %convolution_convert_fusion.2 = bf16[256,64]{0,1:T(8,128)(2,1)S(1)} fusion(bf16[256,2048]{1,0:T(8,128)(2,1)} %all-gather.3.cloned.1.call-done, bf16[2048,64]{0,1:T(8,128)(2,1)} %param.13), kind=kOutput, calls=%fused_computation.29 | convolution fusion | flops 67125248 | bytes 1343488 | tf_op jit(solution)/shard_map/dot_general | solution.py:14
  41.2 1.7 %convolution_convert_fusion.3 = bf16[256,64]{0,1:T(8,128)(2,1)S(1)} fusion(bf16[256,2048]{1,0:T(8,128)(2,1)} %all-gather.3.cloned.1.call-done, bf16[2048,64]{0,1:T(8,128)(2,1)} %param.12), kind=kOutput, calls=%fused_computation.30 | convolution fusion | flops 67125248 | bytes 1343488 | tf_op jit(solution)/shard_map/dot_general | solution.py:13
  42.9 31.4 %all_gather.13 = bf16[2048,128]{0,1:T(8,128)(2,1)S(1)} all-gather(bf16[256,128]{0,1:T(8,128)(2,1)S(1)} %pad_maximum_fusion), channel_id=1, replica_groups=mesh['sp'=8,'tp'=4] {'sp'}, dimensions={0}, use_global_device_ids=true | all-gather | bytes 589824 | tf_op jit(solution)/shard_map/all_gather | solution.py:48
  74.2 1.7 %convolution_convert_fusion.1 = bf16[256,256]{0,1:T(8,128)(2,1)S(1)} fusion(bf16[256,2048]{1,0:T(8,128)(2,1)} %all-gather.3.cloned.1.call-done, bf16[2048,256]{1,0:T(8,128)(2,1)S(1)} %copy-done), kind=kOutput, calls=%fused_computation.28 | convolution fusion | flops 268500992 | bytes 2228224 | tf_op jit(solution)/shard_map/dot_general | solution.py:12
  76.1 17.2 %while.18 = (s32[]{:T(128)}, f32[1,4,256]{2,1,0:T(4,128)S(1)}, f32[1,4,256]{2,1,0:T(4,128)S(1)}, f32[1,4,256,64]{2,3,1,0:T(8,128)S(1)}, s32[]{:T(128)}, /*index=...) while((s32[]{:T(128)}, f32[1,4,256]{2,1,0:T(4,128)S(1)}, ...), condition=%wide.region_6.7_spmd.clone, body=%wide.region_1.6_spmd.clone.sunk | while | flops 286658816 | bytes 31506816 | solution.py:93
  76.8 7.9 %conditional.3 = ((f32[1,4,256]{2,1,0:T(4,128)S(1)}, f32[1,4,256]{2,1,0:T(4,128)S(1)}, f32[1,4,256,64]{2,3,1,0:T(8,128)S(1)})) conditional(s32[]{:T(128)} %convert_element_type.50, (f32[1,4,256]{2,1,0:T(4,128)S(1)}, f32[1,4,256]{2,1,0:T(4,128)S(1)}, f32[1,4,256,64]{2,3,1,0:T(8,128)S(1)}) %tuple.53, (s32[]{:T(128)}, s32[1024]{0:T(1024)S(1)}, ...), branch_computations={%region_2.0_spmd, %region_3.5_spmd} | conditional | flops 286658816 | bytes 31501442 | solution.py:90
  76.8 0.2 broadcast_compare_fusion
  77.0 2.7 %fusion.5 = (f32[4,256]{1,0:T(4,128)S(1)}, f32[1024,256,4]{1,0,2:T(8,128)}) fusion(f32[4,1024]{1,0:T(4,128)S(1)} %constant_dynamic-slice_fusion, f32[4,256]{1,0:T(4,128)S(1)} %bitcast.78, pred[256,1024]{0,1:T(8,128)(4,1)S(1)} %broadcast_compare_fusion, bf16[256,1,4,64]{0,3,2,1:T(8,128)(2,1)S(1)} %get-tuple-element.293, ...), kind=kOutput, calls=%fused_computation.6 | convolution fusion | flops 139459584 | bytes 4743172 | tf_op jit(solution)/shard_map/while/body/eval_jaxpr/cond/branch_1_fun/tkgd,skd->kgts/dot_general | solution.py:67
  79.7 3.5 %fusion.13 = f32[1,4,256,64]{2,3,1,0:T(8,128)S(1)} fusion(f32[1024,256,4]{1,0,2:T(8,128)} %get-tuple-element.368, f32[4,256]{1,0:T(4,128)S(1)} %bitcast.72, f32[4,1024]{1,0:T(4,128)S(1)} %constant_dynamic-slice_fusion, f32[4,256]{1,0:T(4,128)S(1)} %bitcast.79, pred[256,1024]{0,1:T(8,128)(4,1)S(1)} %broadcast_compare_fusion, ...), kind=kOutput, calls=%fused_computation.11 | convolution fusion | flops 140640256 | bytes 5140488 | tf_op jit(solution)/shard_map/while/body/eval_jaxpr/cond/branch_1_fun/kgts,skd->kgtd/dot_general | solution.py:78
  83.2 1.4 %fusion.4 = f32[4,256]{1,0:T(4,128)S(1)} fusion(f32[1024,256,4]{1,0,2:T(8,128)S(1)} %copy-done.1, f32[4,256]{1,0:T(4,128)S(1)} %bitcast.73, f32[4,1024]{1,0:T(4,128)S(1)} %constant_dynamic-slice_fusion, f32[4,256]{1,0:T(4,128)S(1)} %bitcast.80, pred[256,1024]{0,1:T(8,128)(4,1)S(1)} %broadcast_compare_fusion), kind=kLoop, calls=%fused_computation.5 | loop fusion | flops 6290432 | bytes 4485120 | tf_op jit(solution)/shard_map/while/body/eval_jaxpr/cond/branch_1_fun/reduce_sum | solution.py:77
  85.3 7.9 %conditional.3 = ((f32[1,4,256]{2,1,0:T(4,128)S(1)}, f32[1,4,256]{2,1,0:T(4,128)S(1)}, f32[1,4,256,64]{2,3,1,0:T(8,128)S(1)})) conditional(s32[]{:T(128)} %convert_element_type.50, (f32[1,4,256]{2,1,0:T(4,128)S(1)}, f32[1,4,256]{2,1,0:T(4,128)S(1)}, f32[1,4,256,64]{2,3,1,0:T(8,128)S(1)}) %tuple.53, (s32[]{:T(128)}, s32[1024]{0:T(1024)S(1)}, ...), branch_computations={%region_2.0_spmd, %region_3.5_spmd} | conditional | flops 286658816 | bytes 31501442 | solution.py:90
  85.4 0.2 broadcast_compare_fusion
  85.6 2.7 %fusion.5 = (f32[4,256]{1,0:T(4,128)S(1)}, f32[1024,256,4]{1,0,2:T(8,128)}) fusion(f32[4,1024]{1,0:T(4,128)S(1)} %constant_dynamic-slice_fusion, f32[4,256]{1,0:T(4,128)S(1)} %bitcast.78, pred[256,1024]{0,1:T(8,128)(4,1)S(1)} %broadcast_compare_fusion, bf16[256,1,4,64]{0,3,2,1:T(8,128)(2,1)S(1)} %get-tuple-element.293, ...), kind=kOutput, calls=%fused_computation.6 | convolution fusion | flops 139459584 | bytes 4743172 | tf_op jit(solution)/shard_map/while/body/eval_jaxpr/cond/branch_1_fun/tkgd,skd->kgts/dot_general | solution.py:67
  88.3 3.5 %fusion.13 = f32[1,4,256,64]{2,3,1,0:T(8,128)S(1)} fusion(f32[1024,256,4]{1,0,2:T(8,128)} %get-tuple-element.368, f32[4,256]{1,0:T(4,128)S(1)} %bitcast.72, f32[4,1024]{1,0:T(4,128)S(1)} %constant_dynamic-slice_fusion, f32[4,256]{1,0:T(4,128)S(1)} %bitcast.79, pred[256,1024]{0,1:T(8,128)(4,1)S(1)} %broadcast_compare_fusion, ...), kind=kOutput, calls=%fused_computation.11 | convolution fusion | flops 140640256 | bytes 5140488 | tf_op jit(solution)/shard_map/while/body/eval_jaxpr/cond/branch_1_fun/kgts,skd->kgtd/dot_general | solution.py:78
  91.8 1.4 %fusion.4 = f32[4,256]{1,0:T(4,128)S(1)} fusion(f32[1024,256,4]{1,0,2:T(8,128)S(1)} %copy-done.1, f32[4,256]{1,0:T(4,128)S(1)} %bitcast.73, f32[4,1024]{1,0:T(4,128)S(1)} %constant_dynamic-slice_fusion, f32[4,256]{1,0:T(4,128)S(1)} %bitcast.80, pred[256,1024]{0,1:T(8,128)(4,1)S(1)} %broadcast_compare_fusion), kind=kLoop, calls=%fused_computation.5 | loop fusion | flops 6290432 | bytes 4485120 | tf_op jit(solution)/shard_map/while/body/eval_jaxpr/cond/branch_1_fun/reduce_sum | solution.py:77
  93.3 0.2 reshape.96
  93.4 0.2 copy.12
  93.6 7.3 %all_to_all.19 = bf16[4,64,256]{2,1,0:T(8,128)(2,1)S(1)} all-to-all(bf16[4,64,256]{2,1,0:T(8,128)(2,1)S(1)} %copy.12), channel_id=1, replica_groups=mesh['sp'=8,'tp'=4] {'tp'}, dimensions={0} | all-to-all | bytes 262144 | tf_op jit(solution)/shard_map/all_to_all | solution.py:100
  100.9 3.7 %convolution_convert_fusion = bf16[64,2048]{1,0:T(8,128)(2,1)} fusion(bf16[64,1024]{1,0:T(8,128)(2,1)S(1)} %bitcast.74, bf16[1024,2048]{1,0:T(8,128)(2,1)} %all-gather.5.cloned.1.call-done), kind=kOutput, calls=%fused_computation.27 | convolution fusion | flops 268566528 | bytes 4587520 | tf_op jit(solution)/shard_map/dot_general | solution.py:101
  (33 shorter events, 0.2 us)
Async XLA Ops:
  6.5 67.7 %copy-start = (bf16[2048,256]{1,0:T(8,128)(2,1)S(1)}, bf16[2048,256]{1,0:T(8,128)(2,1)}, u32[]{:S(2)}) copy-start(bf16[2048,256]{1,0:T(8,128)(2,1)} %param.11) | copy-start | bytes 3145732
  6.5 69.5 %copy-start.2 = (f32[4,256]{1,0:T(4,128)S(1)}, f32[4,256]{1,0:T(4,128)}, u32[]{:S(2)}) copy-start(f32[4,256]{1,0:T(4,128)} %param.15) | copy-start | bytes 12292
  6.5 32.9 %all-gather.3.cloned.1.call-start = ((), (), s32[]{:S(2)}) async-start(), calls=%async_computation.1 | async-start | bytes 1310720 | tf_op jit(solution)/shard_map/all_gather | solution.py:11
  7.3 93.6 %all-gather.5.cloned.1.call-start = ((), (), s32[]{:S(2)}) async-start(), calls=%async_computation.2 | async-start | bytes 5242880 | tf_op jit(solution)/shard_map/all_gather | solution.py:103
  79.7 3.5 %copy-start.1 = (f32[1024,256,4]{1,0,2:T(8,128)S(1)}, f32[1024,256,4]{1,0,2:T(8,128)}, u32[]{:S(2)}) copy-start(f32[1024,256,4]{1,0,2:T(8,128)} %get-tuple-element.368) | copy-start | bytes 12582916 | tf_op jit(solution)/shard_map/while/body/eval_jaxpr/cond
  88.3 3.5 %copy-start.1 = (f32[1024,256,4]{1,0,2:T(8,128)S(1)}, f32[1024,256,4]{1,0,2:T(8,128)}, u32[]{:S(2)}) copy-start(f32[1024,256,4]{1,0,2:T(8,128)} %get-tuple-element.368) | copy-start | bytes 12582916 | tf_op jit(solution)/shard_map/while/body/eval_jaxpr/cond
Sparse Core Ops, SparseCore 0:
  8.9 17.6 all-gather.2
  28.1 34.4 all-gather.4
where the time goes:
time: 112 us; the launch traced here: 111 us
  blocking collectives  69.4 us (62%)
  matrix products  21.2 us (19%)
  between operations  13.5 us (12%)
  other arithmetic  3.96 us (4%)
  loops' own time  1.6 us (1%)
  waiting for transfers between devices  1.43 us (1%)
    all_gather x1, blocking collectives, per_device(): pieces = lax.all_gather(key_values, 'sp', axis=0, tiled=True)  31.4 us
    all_gather x1, blocking collectives, per_device(): gate_all = lax.all_gather(cum_gate, 'sp', axis=1, tiled=True)  30.7 us
    all_to_all x1, blocking collectives, per_device(): lax.all_to_all(attended, 'tp', split_axis=0, concat_axis=1, tiled=True)  7.26 us
    dot_general x2, matrix products, compute(): jnp.einsum('kgts,skd->kgtd', weights.astype(jnp.bfloat16), value_rows, pr...  6.97 us
    dot_general x2, matrix products, compute(): jnp.einsum('tkgd,skd->kgts', queries, key_rows, preferred_element_type=jn...  5.33 us
    dot_general x1, matrix products, per_device(): jnp.dot(regrouped, lax.all_gather(w_out, 'tp', axis=0, tiled=True), prefe...  3.74 us
    reduce_sum x2, other arithmetic, compute(): weight_sum = weight_sum * decay + jnp.sum(weights, axis=-1)  2.74 us
  transfers between devices with their start and end apart: 2, of which 0 were waited for; matrix products, arithmetic and copies ran while one was open for 20% of the time, Pallas kernels for 0%

commit v1 on v0

--- a/solution.py
+++ b/solution.py
@@ -45,7 +45,12 @@
             for member in prepared
         )
     )
-    pieces = lax.all_gather(key_values, "sp", axis=0, tiled=True)
+    ring = [key_values]
+    for hop in range(7):
+        ring.append(lax.ppermute(ring[-1], "sp", [(dev, (dev + 1) % 8) for dev in range(8)]))
+    pieces = jnp.roll(
+        jnp.concatenate(ring[::-1], axis=0), (lax.axis_index("sp") + 1) * ring[0].shape[0], axis=0
+    )
     piece_rows = pieces.shape[0]
     key_block = math.gcd(piece_rows, 1024)
 

time: 112 us -> 137 us (1.22)
  waiting for transfers between devices: 1.43 us -> 33.9 us
  blocking collectives: 69.4 us -> 37.7 us
  starting transfers between devices: 0.04 us -> 24.2 us
    all_gather x1 -> x0, blocking collectives: 31.4 us -> none  [per_device(): pieces = lax.all_gather(key_values, 'sp', axis=0, tiled=True)]
    ppermute x0 -> x7, starting transfers between devices: none -> 24.2 us  [per_device(): lax.ppermute(ring[-1], 'sp', [(dev, (dev + 1) % 8) for dev in range(8)])]
    all_gather x1, waiting for transfers between devices: 0.01 us -> 18.6 us  [per_device(): pieces = lax.all_gather(tokens, 'tp', axis=0, tiled=True)]
    ppermute x0 -> x7, waiting for transfers between devices: none -> 13.9 us  [per_device(): lax.ppermute(ring[-1], 'sp', [(dev, (dev + 1) % 8) for dev in range(8)])]
  transfers between devices with their start and end apart: 2 -> 9, of which waited for: 0 -> 7; matrix products, arithmetic and copies ran while one was open for 20% -> 16% of each run, Pallas kernels for 0% -> 0%
where the time goes in v1:
time: 137 us; the launch traced here: 136 us
  blocking collectives  37.7 us (28%)
  waiting for transfers between devices  33.9 us (25%)
  starting transfers between devices  24.2 us (18%)
  matrix products  21.2 us (15%)
  between operations  13.6 us (10%)
  other arithmetic  3.9 us (3%)
  loops' own time  1.37 us (1%)
    all_gather x1, blocking collectives, per_device(): gate_all = lax.all_gather(cum_gate, 'sp', axis=1, tiled=True)  30.7 us
    ppermute x7, starting transfers between devices, per_device(): lax.ppermute(ring[-1], 'sp', [(dev, (dev + 1) % 8) for dev in range(8)])  24.2 us
    all_gather x1, waiting for transfers between devices, per_device(): pieces = lax.all_gather(tokens, 'tp', axis=0, tiled=True)  18.6 us
    ppermute x7, waiting for transfers between devices, per_device(): lax.ppermute(ring[-1], 'sp', [(dev, (dev + 1) % 8) for dev in range(8)])  13.9 us
    all_to_all x1, blocking collectives, per_device(): lax.all_to_all(attended, 'tp', split_axis=0, concat_axis=1, tiled=True)  6.99 us
    dot_general x2, matrix products, compute(): jnp.einsum('kgts,skd->kgtd', weights.astype(jnp.bfloat16), value_rows, pr...  6.97 us
    dot_general x2, matrix products, compute(): jnp.einsum('tkgd,skd->kgts', queries, key_rows, preferred_element_type=jn...  5.32 us
    dot_general x1, matrix products, per_device(): jnp.dot(regrouped, lax.all_gather(w_out, 'tp', axis=0, tiled=True), prefe...  3.74 us
  transfers between devices with their start and end apart: 9, of which 7 were waited for; matrix products, arithmetic and copies ran while one was open for 16% of the time, Pallas kernels for 0%

profile of v1, /device:TPU:26, one launch (start us, length us, event | category | flops | bytes accessed | tf_op | source)
XLA Modules:
  0.0 136.5 jit_solution(2070109648422890594)
XLA Ops:
  8.0 18.6 %all-gather.3.cloned.1.call-done = bf16[256,2048]{1,0:T(8,128)(2,1)} async-done(((bf16[64,2048]{1,0:T(8,128)(2,1)}), bf16[256,2048]{1,0:T(8,128)(2,1)}) %all-gather.3.cloned.1.call-update) | async-done | bytes 1048592 | tf_op jit(solution)/shard_map/all_gather | solution.py:11
  28.3 1.7 %convolution_convert_fusion.3 = bf16[256,64]{0,1:T(8,128)(2,1)S(1)} fusion(bf16[256,2048]{1,0:T(8,128)(2,1)} %all-gather.3.cloned.1.call-done, bf16[2048,64]{0,1:T(8,128)(2,1)} %param.12), kind=kOutput, calls=%fused_computation.30 | convolution fusion | flops 67125248 | bytes 1343488 | tf_op jit(solution)/shard_map/dot_general | solution.py:13
  30.6 3.8 %collective-permute-done = bf16[256,128]{0,1:T(8,128)(2,1)S(1)} collective-permute-done((bf16[256,128]{0,1:T(8,128)(2,1)S(1)}, bf16[256,128]{0,1:T(8,128)(2,1)S(1)}, u32[]{:S(2)}, u32[]{:S(2)}) %collective-permute-start) | collective-permute-done | bytes 65568 | tf_op jit(solution)/shard_map/ppermute | solution.py:50
  34.3 3.2 %collective-permute-start.1 = (bf16[256,128]{0,1:T(8,128)(2,1)S(1)}, bf16[256,128]{0,1:T(8,128)(2,1)S(1)}, u32[]{:S(2)}, u32[]{:S(2)}) collective-permute-start(bf16[256,128]{0,1:T(8,128)(2,1)S(1)} %collective-permute-done), channel_id=1, source_target_pairs={{0,4},{4,8},{8,12},{12,16},{16,20},{20,24},{24,28},{28,0},{1,5},{5... | collective-permute-start | bytes 196616 | tf_op jit(solution)/shard_map/ppermute | solution.py:50
  37.5 1.9 %collective-permute-done.1 = bf16[256,128]{0,1:T(8,128)(2,1)S(1)} collective-permute-done((bf16[256,128]{0,1:T(8,128)(2,1)S(1)}, bf16[256,128]{0,1:T(8,128)(2,1)S(1)}, u32[]{:S(2)}, u32[]{:S(2)}) %collective-permute-start.1) | collective-permute-done | bytes 65568 | tf_op jit(solution)/shard_map/ppermute | solution.py:50
  39.4 5.1 %collective-permute-start.2 = (bf16[256,128]{0,1:T(8,128)(2,1)S(1)}, bf16[256,128]{0,1:T(8,128)(2,1)S(1)}, u32[]{:S(2)}, u32[]{:S(2)}) collective-permute-start(bf16[256,128]{0,1:T(8,128)(2,1)S(1)} %collective-permute-done.1), channel_id=1, source_target_pairs={{0,4},{4,8},{8,12},{12,16},{16,20},{20,24},{24,28},{28,0},{1,5},{5... | collective-permute-start | bytes 196616 | tf_op jit(solution)/shard_map/ppermute | solution.py:50
  44.5 1.9 %collective-permute-done.2 = bf16[256,128]{0,1:T(8,128)(2,1)S(1)} collective-permute-done((bf16[256,128]{0,1:T(8,128)(2,1)S(1)}, bf16[256,128]{0,1:T(8,128)(2,1)S(1)}, u32[]{:S(2)}, u32[]{:S(2)}) %collective-permute-start.2) | collective-permute-done | bytes 65568 | tf_op jit(solution)/shard_map/ppermute | solution.py:50
  46.4 5.1 %collective-permute-start.3 = (bf16[256,128]{0,1:T(8,128)(2,1)S(1)}, bf16[256,128]{0,1:T(8,128)(2,1)S(1)}, u32[]{:S(2)}, u32[]{:S(2)}) collective-permute-start(bf16[256,128]{0,1:T(8,128)(2,1)S(1)} %collective-permute-done.2), channel_id=1, source_target_pairs={{0,4},{4,8},{8,12},{12,16},{16,20},{20,24},{24,28},{28,0},{1,5},{5... | collective-permute-start | bytes 196616 | tf_op jit(solution)/shard_map/ppermute | solution.py:50
  51.4 1.9 %collective-permute-done.3 = bf16[256,128]{0,1:T(8,128)(2,1)S(1)} collective-permute-done((bf16[256,128]{0,1:T(8,128)(2,1)S(1)}, bf16[256,128]{0,1:T(8,128)(2,1)S(1)}, u32[]{:S(2)}, u32[]{:S(2)}) %collective-permute-start.3) | collective-permute-done | bytes 65568 | tf_op jit(solution)/shard_map/ppermute | solution.py:50
  53.4 5.1 %collective-permute-start.4 = (bf16[256,128]{0,1:T(8,128)(2,1)S(1)}, bf16[256,128]{0,1:T(8,128)(2,1)S(1)}, u32[]{:S(2)}, u32[]{:S(2)}) collective-permute-start(bf16[256,128]{0,1:T(8,128)(2,1)S(1)} %collective-permute-done.3), channel_id=1, source_target_pairs={{0,4},{4,8},{8,12},{12,16},{16,20},{20,24},{24,28},{28,0},{1,5},{5... | collective-permute-start | bytes 196616 | tf_op jit(solution)/shard_map/ppermute | solution.py:50
  58.4 2.0 %collective-permute-done.4 = bf16[256,128]{0,1:T(8,128)(2,1)S(1)} collective-permute-done((bf16[256,128]{0,1:T(8,128)(2,1)S(1)}, bf16[256,128]{0,1:T(8,128)(2,1)S(1)}, u32[]{:S(2)}, u32[]{:S(2)}) %collective-permute-start.4) | collective-permute-done | bytes 65568 | tf_op jit(solution)/shard_map/ppermute | solution.py:50
  60.4 5.2 %collective-permute-start.5 = (bf16[256,128]{0,1:T(8,128)(2,1)S(1)}, bf16[256,128]{0,1:T(8,128)(2,1)S(1)}, u32[]{:S(2)}, u32[]{:S(2)}) collective-permute-start(bf16[256,128]{0,1:T(8,128)(2,1)S(1)} %collective-permute-done.4), channel_id=1, source_target_pairs={{0,4},{4,8},{8,12},{12,16},{16,20},{20,24},{24,28},{28,0},{1,5},{5... | collective-permute-start | bytes 196616 | tf_op jit(solution)/shard_map/ppermute | solution.py:50
  66.2 30.7 %all_gather.10 = f32[4,2048]{1,0:T(4,128)S(1)} all-gather(f32[4,256]{1,0:T(4,128)} %param.15), channel_id=1, replica_groups=mesh['sp'=8,'tp'=4] {'sp'}, dimensions={1}, use_global_device_ids=true | all-gather | bytes 36864 | tf_op jit(solution)/shard_map/all_gather | solution.py:25
  97.0 1.7 %convolution_convert_fusion.1 = bf16[256,256]{0,1:T(8,128)(2,1)S(1)} fusion(bf16[256,2048]{1,0:T(8,128)(2,1)} %all-gather.3.cloned.1.call-done, bf16[2048,256]{1,0:T(8,128)(2,1)S(1)} %copy-done), kind=kOutput, calls=%fused_computation.28 | convolution fusion | flops 268500992 | bytes 2228224 | tf_op jit(solution)/shard_map/dot_general | solution.py:12
  98.8 2.4 %collective-permute-done.6 = bf16[256,128]{0,1:T(8,128)(2,1)S(1)} collective-permute-done((bf16[256,128]{0,1:T(8,128)(2,1)S(1)}, bf16[256,128]{0,1:T(8,128)(2,1)S(1)}, u32[]{:S(2)}, u32[]{:S(2)}) %collective-permute-start.6) | collective-permute-done | bytes 65568 | tf_op jit(solution)/shard_map/ppermute | solution.py:50
  101.6 16.9 %while.18 = (s32[]{:T(128)}, f32[1,4,256]{2,1,0:T(4,128)S(1)}, f32[1,4,256]{2,1,0:T(4,128)S(1)}, f32[1,4,256,64]{2,3,1,0:T(8,128)S(1)}, s32[]{:T(128)}, /*index=...) while((s32[]{:T(128)}, f32[1,4,256]{2,1,0:T(4,128)S(1)}, ...), condition=%wide.region_6.7_spmd.clone, body=%wide.region_1.6_spmd.clone.sunk | while | flops 286658816 | bytes 31506816 | solution.py:98
  102.1 7.9 %conditional.3 = ((f32[1,4,256]{2,1,0:T(4,128)S(1)}, f32[1,4,256]{2,1,0:T(4,128)S(1)}, f32[1,4,256,64]{2,3,1,0:T(8,128)S(1)})) conditional(s32[]{:T(128)} %convert_element_type.50, (f32[1,4,256]{2,1,0:T(4,128)S(1)}, f32[1,4,256]{2,1,0:T(4,128)S(1)}, f32[1,4,256,64]{2,3,1,0:T(8,128)S(1)}) %tuple.53, (s32[]{:T(128)}, s32[1024]{0:T(1024)S(1)}, ...), branch_computations={%region_2.2_spmd, %region_3.5_spmd} | conditional | flops 286658816 | bytes 31501442 | solution.py:95
  102.4 2.7 %fusion.5 = (f32[4,256]{1,0:T(4,128)S(1)}, f32[1024,256,4]{1,0,2:T(8,128)}) fusion(f32[4,1024]{1,0:T(4,128)S(1)} %constant_dynamic-slice_fusion, f32[4,256]{1,0:T(4,128)S(1)} %bitcast.78, pred[256,1024]{0,1:T(8,128)(4,1)S(1)} %broadcast_compare_fusion, bf16[256,1,4,64]{0,3,2,1:T(8,128)(2,1)S(1)} %get-tuple-element.293, ...), kind=kOutput, calls=%fused_computation.6 | convolution fusion | flops 139459584 | bytes 4743172 | tf_op jit(solution)/shard_map/while/body/eval_jaxpr/cond/branch_1_fun/tkgd,skd->kgts/dot_general | solution.py:72
  105.1 3.5 %fusion.13 = f32[1,4,256,64]{2,3,1,0:T(8,128)S(1)} fusion(f32[1024,256,4]{1,0,2:T(8,128)} %get-tuple-element.368, f32[4,256]{1,0:T(4,128)S(1)} %bitcast.72, f32[4,1024]{1,0:T(4,128)S(1)} %constant_dynamic-slice_fusion, f32[4,256]{1,0:T(4,128)S(1)} %bitcast.79, pred[256,1024]{0,1:T(8,128)(4,1)S(1)} %broadcast_compare_fusion, ...), kind=kOutput, calls=%fused_computation.11 | convolution fusion | flops 140640256 | bytes 5140488 | tf_op jit(solution)/shard_map/while/body/eval_jaxpr/cond/branch_1_fun/kgts,skd->kgtd/dot_general | solution.py:83
  110.6 7.9 %conditional.3 = ((f32[1,4,256]{2,1,0:T(4,128)S(1)}, f32[1,4,256]{2,1,0:T(4,128)S(1)}, f32[1,4,256,64]{2,3,1,0:T(8,128)S(1)})) conditional(s32[]{:T(128)} %convert_element_type.50, (f32[1,4,256]{2,1,0:T(4,128)S(1)}, f32[1,4,256]{2,1,0:T(4,128)S(1)}, f32[1,4,256,64]{2,3,1,0:T(8,128)S(1)}) %tuple.53, (s32[]{:T(128)}, s32[1024]{0:T(1024)S(1)}, ...), branch_computations={%region_2.2_spmd, %region_3.5_spmd} | conditional | flops 286658816 | bytes 31501442 | solution.py:95
  110.9 2.7 %fusion.5 = (f32[4,256]{1,0:T(4,128)S(1)}, f32[1024,256,4]{1,0,2:T(8,128)}) fusion(f32[4,1024]{1,0:T(4,128)S(1)} %constant_dynamic-slice_fusion, f32[4,256]{1,0:T(4,128)S(1)} %bitcast.78, pred[256,1024]{0,1:T(8,128)(4,1)S(1)} %broadcast_compare_fusion, bf16[256,1,4,64]{0,3,2,1:T(8,128)(2,1)S(1)} %get-tuple-element.293, ...), kind=kOutput, calls=%fused_computation.6 | convolution fusion | flops 139459584 | bytes 4743172 | tf_op jit(solution)/shard_map/while/body/eval_jaxpr/cond/branch_1_fun/tkgd,skd->kgts/dot_general | solution.py:72
  113.6 3.5 %fusion.13 = f32[1,4,256,64]{2,3,1,0:T(8,128)S(1)} fusion(f32[1024,256,4]{1,0,2:T(8,128)} %get-tuple-element.368, f32[4,256]{1,0:T(4,128)S(1)} %bitcast.72, f32[4,1024]{1,0:T(4,128)S(1)} %constant_dynamic-slice_fusion, f32[4,256]{1,0:T(4,128)S(1)} %bitcast.79, pred[256,1024]{0,1:T(8,128)(4,1)S(1)} %broadcast_compare_fusion, ...), kind=kOutput, calls=%fused_computation.11 | convolution fusion | flops 140640256 | bytes 5140488 | tf_op jit(solution)/shard_map/while/body/eval_jaxpr/cond/branch_1_fun/kgts,skd->kgtd/dot_general | solution.py:83
  118.9 7.0 %all_to_all.19 = bf16[4,64,256]{2,1,0:T(8,128)(2,1)S(1)} all-to-all(bf16[4,64,256]{2,1,0:T(8,128)(2,1)S(1)} %copy.12), channel_id=1, replica_groups=mesh['sp'=8,'tp'=4] {'tp'}, dimensions={0} | all-to-all | bytes 262144 | tf_op jit(solution)/shard_map/all_to_all | solution.py:105
  125.9 3.7 %convolution_convert_fusion = bf16[64,2048]{1,0:T(8,128)(2,1)} fusion(bf16[64,1024]{1,0:T(8,128)(2,1)S(1)} %bitcast.74, bf16[1024,2048]{1,0:T(8,128)(2,1)} %all-gather.5.cloned.1.call-done), kind=kOutput, calls=%fused_computation.27 | convolution fusion | flops 268566528 | bytes 4587520 | tf_op jit(solution)/shard_map/dot_general | solution.py:106
  (63 shorter events, 8.2 us)
Async XLA Ops:
  6.5 90.5 %copy-start = (bf16[2048,256]{1,0:T(8,128)(2,1)S(1)}, bf16[2048,256]{1,0:T(8,128)(2,1)}, u32[]{:S(2)}) copy-start(bf16[2048,256]{1,0:T(8,128)(2,1)} %param.11) | copy-start | bytes 3145732
  6.5 20.0 %all-gather.3.cloned.1.call-start = ((), (), s32[]{:S(2)}) async-start(), calls=%async_computation.1 | async-start | bytes 1310720 | tf_op jit(solution)/shard_map/all_gather | solution.py:11
  7.3 118.6 %all-gather.5.cloned.1.call-start = ((), (), s32[]{:S(2)}) async-start(), calls=%async_computation.2 | async-start | bytes 5242880 | tf_op jit(solution)/shard_map/all_gather | solution.py:108
  8.0 93.5 %copy-start.2 = (f32[4,256]{1,0:T(4,128)S(1)}, f32[4,256]{1,0:T(4,128)}, u32[]{:S(2)}) copy-start(f32[4,256]{1,0:T(4,128)} %param.15) | copy-start | bytes 12292
  30.0 4.3 %collective-permute-start = (bf16[256,128]{0,1:T(8,128)(2,1)S(1)}, bf16[256,128]{0,1:T(8,128)(2,1)S(1)}, u32[]{:S(2)}, u32[]{:S(2)}) collective-permute-start(bf16[256,128]{0,1:T(8,128)(2,1)S(1)} %pad_maximum_fusion), channel_id=1, source_target_pairs={{0,4},{4,8},{8,12},{12,16},{16,20},{20,24},{24,28},{28,0},{1,5},{5... | collective-permute-start | bytes 196616 | tf_op jit(solution)/shard_map/ppermute | solution.py:50
  34.3 5.1 %collective-permute-start.1 = (bf16[256,128]{0,1:T(8,128)(2,1)S(1)}, bf16[256,128]{0,1:T(8,128)(2,1)S(1)}, u32[]{:S(2)}, u32[]{:S(2)}) collective-permute-start(bf16[256,128]{0,1:T(8,128)(2,1)S(1)} %collective-permute-done), channel_id=1, source_target_pairs={{0,4},{4,8},{8,12},{12,16},{16,20},{20,24},{24,28},{28,0},{1,5},{5... | collective-permute-start | bytes 196616 | tf_op jit(solution)/shard_map/ppermute | solution.py:50
  39.4 7.0 %collective-permute-start.2 = (bf16[256,128]{0,1:T(8,128)(2,1)S(1)}, bf16[256,128]{0,1:T(8,128)(2,1)S(1)}, u32[]{:S(2)}, u32[]{:S(2)}) collective-permute-start(bf16[256,128]{0,1:T(8,128)(2,1)S(1)} %collective-permute-done.1), channel_id=1, source_target_pairs={{0,4},{4,8},{8,12},{12,16},{16,20},{20,24},{24,28},{28,0},{1,5},{5... | collective-permute-start | bytes 196616 | tf_op jit(solution)/shard_map/ppermute | solution.py:50
  46.4 7.0 %collective-permute-start.3 = (bf16[256,128]{0,1:T(8,128)(2,1)S(1)}, bf16[256,128]{0,1:T(8,128)(2,1)S(1)}, u32[]{:S(2)}, u32[]{:S(2)}) collective-permute-start(bf16[256,128]{0,1:T(8,128)(2,1)S(1)} %collective-permute-done.2), channel_id=1, source_target_pairs={{0,4},{4,8},{8,12},{12,16},{16,20},{20,24},{24,28},{28,0},{1,5},{5... | collective-permute-start | bytes 196616 | tf_op jit(solution)/shard_map/ppermute | solution.py:50
  53.4 7.1 %collective-permute-start.4 = (bf16[256,128]{0,1:T(8,128)(2,1)S(1)}, bf16[256,128]{0,1:T(8,128)(2,1)S(1)}, u32[]{:S(2)}, u32[]{:S(2)}) collective-permute-start(bf16[256,128]{0,1:T(8,128)(2,1)S(1)} %collective-permute-done.3), channel_id=1, source_target_pairs={{0,4},{4,8},{8,12},{12,16},{16,20},{20,24},{24,28},{28,0},{1,5},{5... | collective-permute-start | bytes 196616 | tf_op jit(solution)/shard_map/ppermute | solution.py:50
  60.4 36.5 %collective-permute-start.5 = (bf16[256,128]{0,1:T(8,128)(2,1)S(1)}, bf16[256,128]{0,1:T(8,128)(2,1)S(1)}, u32[]{:S(2)}, u32[]{:S(2)}) collective-permute-start(bf16[256,128]{0,1:T(8,128)(2,1)S(1)} %collective-permute-done.4), channel_id=1, source_target_pairs={{0,4},{4,8},{8,12},{12,16},{16,20},{20,24},{24,28},{28,0},{1,5},{5... | collective-permute-start | bytes 196616 | tf_op jit(solution)/shard_map/ppermute | solution.py:50
  97.0 4.3 %collective-permute-start.6 = (bf16[256,128]{0,1:T(8,128)(2,1)S(1)}, bf16[256,128]{0,1:T(8,128)(2,1)S(1)}, u32[]{:S(2)}, u32[]{:S(2)}) collective-permute-start(bf16[256,128]{0,1:T(8,128)(2,1)S(1)} %collective-permute-done.5), channel_id=1, source_target_pairs={{0,4},{4,8},{8,12},{12,16},{16,20},{20,24},{24,28},{28,0},{1,5},{5... | collective-permute-start | bytes 196616 | tf_op jit(solution)/shard_map/ppermute | solution.py:50
  105.1 3.5 %copy-start.1 = (f32[1024,256,4]{1,0,2:T(8,128)S(1)}, f32[1024,256,4]{1,0,2:T(8,128)}, u32[]{:S(2)}) copy-start(f32[1024,256,4]{1,0,2:T(8,128)} %get-tuple-element.368) | copy-start | bytes 12582916 | tf_op jit(solution)/shard_map/while/body/eval_jaxpr/cond
  113.6 3.5 %copy-start.1 = (f32[1024,256,4]{1,0,2:T(8,128)S(1)}, f32[1024,256,4]{1,0,2:T(8,128)}, u32[]{:S(2)}) copy-start(f32[1024,256,4]{1,0,2:T(8,128)} %get-tuple-element.368) | copy-start | bytes 12582916 | tf_op jit(solution)/shard_map/while/body/eval_jaxpr/cond
Sparse Core Ops, SparseCore 0:
  8.9 17.6 all-gather.2
  28.1 34.4 all-gather.4
